TPU v7x, 32 devices: a whole 2x2x4 slice. The times are simulated.
32 devices in a mesh: kv: 4 (over y, x), tp: 8 (over z, core).
Axes of the slice: x: 2, y: 2, z: 4, core: 2. Of those that a mesh axis runs over, the one named last changes fastest.
Arguments:
- stream: bfloat16 [32, 4096], P(None, ('kv', 'tp')), may hold values from -18 to 18
- mixer_gain: float32 [4096], replicated, may hold values from 0.1 to 1.9
- query_weight: bfloat16 [4096, 1024], P(None, 'tp'), may hold values from -0.09375 to 0.09375
- key_weight: bfloat16 [4096, 1024], P(None, 'tp'), may hold values from -0.09375 to 0.09375
- value_weight: bfloat16 [4096, 1024], P(None, 'tp'), may hold values from -0.09375 to 0.09375
- forget_weight: bfloat16 [4096, 16], replicated, may hold values from -0.09375 to 0.09375
- forget_bias: float32 [16], replicated, may hold values from -4 to -2
- key_cache: bfloat16 [32, 16, 4096, 64], P(None, 'tp', 'kv'), may hold values from -512 to 512, as said below
- value_cache: bfloat16 [32, 16, 4096, 64], P(None, 'tp', 'kv'), may hold values from -12 to 12
- past_decay: float32 [32, 16, 4096], P(None, 'tp', 'kv'), may hold values from -4096 to 0, as said below
- out_weight: bfloat16 [1024, 4096], P('tp', 'kv'), may hold values from -0.75 to 0.75
- channel_gain: float32 [4096], replicated, may hold values from 0.1 to 1.9
- up_weight: bfloat16 [4096, 16384], P('kv', 'tp'), may hold values from -0.09375 to 0.09375
- down_weight: bfloat16 [16384, 4096], P('tp', 'kv'), may hold values from -0.0625 to 0.0625
Outputs:
- updated: bfloat16 [32, 4096], P(None, ('kv', 'tp'))
Inputs may be any that keep to these rules, and one draw needn't show every extreme that they name: `key_cache`: keys of order one; some cached keys may be much larger. `past_decay`: never falling along the positions of a sequence and head, zero at the last cached position.
All inputs are finite; a program needn't handle non-finite values.
Results may differ from a plain program's by a relative error of at most 0.014.
The roundings to bfloat16 on the way count: a program that leaves them out, or rounds other values in their place, can miss the bound.
Values may be sent and summed in bfloat16 or wider, within the bound.
A program may use at most 64 MiB of HBM per device.

v0:
```python
import jax
import jax.numpy as jnp
from jax import lax
from jax.sharding import PartitionSpec as P

D = 4096


EPS = 1e-06


def combined_all(part, axis, combine):
    gathered = jax.tree.map(lambda a: lax.all_gather(a, axis), part)

    def take(source):
        return jax.tree.map(lambda a: lax.dynamic_index_in_dim(a, source, 0, False), gathered)

    return lax.fori_loop(
        1, lax.axis_size(axis), lambda source, state: combine(state, take(source)), take(0)
    )


def rms_scale(values, gain):
    widened = values.astype(jnp.float32)
    inverse = lax.rsqrt(jnp.mean(widened * widened, axis=-1, keepdims=True) + EPS)
    return (widened * inverse * gain).astype(jnp.bfloat16)


def merge_parts(earlier, later):
    top_one, total_one, sums_one = earlier
    top_two, total_two, sums_two = later
    highest = jnp.maximum(top_one, top_two)
    factor_one = jnp.exp(top_one - highest)
    factor_two = jnp.exp(top_two - highest)
    return (
        highest,
        total_one * factor_one + total_two * factor_two,
        sums_one * factor_one[..., None] + sums_two * factor_two[..., None],
    )


def squared_relu(values):
    return jnp.square(jax.nn.relu(values)).astype(jnp.bfloat16)


def row_squares(values):
    widened = values.astype(jnp.float32)
    return jnp.sum(widened * widened, axis=1)


def shards(
    stream,
    mixer_gain,
    query_weight,
    key_weight,
    value_weight,
    forget_weight,
    forget_bias,
    key_cache,
    value_cache,
    past_decay,
    out_weight,
    channel_gain,
    up_weight,
    down_weight,
):
    batch_rows = stream.shape[0]
    local_heads = key_cache.shape[1]
    head_size = key_cache.shape[3]
    scale_factor = float(head_size) ** (-0.5)
    gathered = lax.all_gather(stream, ("kv", "tp"), axis=1, tiled=True)
    normed = rms_scale(gathered, mixer_gain)
    queries = jnp.dot(normed, query_weight, preferred_element_type=jnp.float32).astype(jnp.bfloat16)
    keys_new = jnp.dot(normed, key_weight, preferred_element_type=jnp.float32).astype(jnp.bfloat16)
    values_new = jnp.dot(normed, value_weight, preferred_element_type=jnp.float32).astype(
        jnp.bfloat16
    )
    forget_all = jax.nn.log_sigmoid(
        jnp.dot(normed, forget_weight, preferred_element_type=jnp.float32) + forget_bias
    )
    forget = lax.dynamic_slice_in_dim(
        forget_all, lax.axis_index("tp") * local_heads, local_heads, 1
    )
    query_heads = queries.reshape(batch_rows, local_heads, head_size)
    scores = (
        jnp.einsum("bhd,bhpd->bhp", query_heads, key_cache, preferred_element_type=jnp.float32)
        * scale_factor
        + forget[..., None]
        + past_decay
    )
    highest = jnp.max(scores, axis=-1)
    weights = jnp.exp(scores - highest[..., None]).astype(jnp.bfloat16)
    totals = jnp.sum(weights.astype(jnp.float32), axis=-1)
    sums = jnp.einsum("bhp,bhpd->bhd", weights, value_cache, preferred_element_type=jnp.float32)
    highest, totals, sums = combined_all((highest, totals, sums), "kv", merge_parts)
    key_heads = keys_new.reshape(batch_rows, local_heads, head_size).astype(jnp.float32)
    value_heads = values_new.reshape(batch_rows, local_heads, head_size).astype(jnp.float32)
    own = jnp.sum(query_heads.astype(jnp.float32) * key_heads, axis=-1) * scale_factor
    peak = jnp.maximum(highest, own)
    cache_factor = jnp.exp(highest - peak)
    own_factor = jnp.exp(own - peak)
    numer = sums * cache_factor[..., None] + value_heads * own_factor[..., None]
    denom = totals * cache_factor + own_factor
    attention = (
        (numer / denom[..., None]).astype(jnp.bfloat16).reshape(batch_rows, local_heads * head_size)
    )
    partial_value = jnp.dot(attention, out_weight, preferred_element_type=jnp.float32)
    piece_width = stream.shape[1]
    block_width = partial_value.shape[1]
    block_sum = lax.psum(partial_value, "tp")
    own_block = lax.dynamic_slice_in_dim(
        gathered, lax.axis_index("kv") * block_width, block_width, 1
    )
    middle_block = (own_block.astype(jnp.float32) + block_sum).astype(jnp.bfloat16)
    squares = lax.psum(row_squares(middle_block), "kv")
    middle_piece = lax.dynamic_slice_in_dim(
        middle_block, lax.axis_index("tp") * piece_width, piece_width, 1
    )
    inverse = lax.rsqrt(squares / D + EPS)
    gain_block = lax.dynamic_slice_in_dim(
        channel_gain, lax.axis_index("kv") * block_width, block_width, 0
    )
    mixed_block = (
        middle_block.astype(jnp.float32) * inverse[:, None] * gain_block[None, :]
    ).astype(jnp.bfloat16)
    up_partial = jnp.dot(mixed_block, up_weight, preferred_element_type=jnp.float32)
    hidden = squared_relu(lax.psum(up_partial, "kv"))
    down_partial = jnp.dot(hidden, down_weight, preferred_element_type=jnp.float32)
    reduced = lax.psum_scatter(down_partial, "tp", scatter_dimension=1, tiled=True)
    return (middle_piece.astype(jnp.float32) + reduced).astype(jnp.bfloat16)


def solution(mesh):
    return jax.shard_map(
        shards,
        mesh=mesh,
        in_specs=(
            P(None, ("kv", "tp")),
            P(),
            P(None, "tp"),
            P(None, "tp"),
            P(None, "tp"),
            P(),
            P(),
            P(None, "tp", "kv", None),
            P(None, "tp", "kv", None),
            P(None, "tp", "kv"),
            P("tp", "kv"),
            P(),
            P("kv", "tp"),
            P("tp", "kv"),
        ),
        out_specs=P(None, ("kv", "tp")),
        check_vma=False,
    )
```

profile of v0, /device:TPU:0, one launch (start us, length us, event | category | flops | bytes accessed | tf_op | source)
XLA Modules:
  0.0 247.9 jit_solution(13276194251928122677)
XLA Ops:
  6.5 0.0 copy-start
  6.5 0.0 all-reduce.3.cloned.1.call-start
  6.5 44.6 %all_gather.21 = bf16[32,4096]{1,0:T(8,128)(2,1)S(1)} all-gather(bf16[32,128]{1,0:T(8,128)(2,1)} %param.16), channel_id=1, replica_groups=mesh['kv'=4,'tp'=8] {'kv','tp'}, dimensions={1}, use_global_device_ids=true | all-gather | bytes 270336 | tf_op jit(solution)/shard_map/all_gather | solution.py:71
  51.2 0.2 fusion.6
  51.3 0.0 copy-done
  51.4 1.0 convolution_convert_fusion.2
  52.4 0.1 reshape.57
  52.5 0.1 reshape.31
  52.6 1.2 fusion.40
  53.8 0.1 copy.32
  53.9 4.6 %fusion.41 = f32[32,2,1,1024]{3,2,1,0:T(1,128)S(1)} fusion(bf16[32,2,64,1]{2,3,1,0:T(2,128)(2,1)S(1)} %reshape.57, bf16[32,2,1024,64]{2,3,1,0:T(8,128)(2,1)} %param.23), kind=kOutput, calls=%fused_computation.63 | convolution fusion | flops 8388608 | bytes 8658944 | tf_op jit(solution)/shard_map/bhd,bhpd->bhp/dot_general | solution.py:86
  58.4 0.0 copy-start.1
  58.4 0.0 copy-start.4
  58.5 0.0 copy-start.2
  58.5 2.1 fusion.38
  60.5 0.1 copy.33
  60.6 1.3 fusion.30
  61.9 5.7 %fusion.11 = f32[32,2,1,64]{3,2,1,0:T(1,128)S(1)} fusion(bf16[32,2,1024,64]{2,3,1,0:T(8,128)(2,1)} %param.24, bf16[32,2,1024,1]{2,1,0,3:T(2,128)(2,1)S(1)} %get-tuple-element.211), kind=kOutput, calls=%fused_computation.24 | convolution fusion | flops 8388608 | bytes 8536064 | tf_op jit(solution)/shard_map/bhp,bhpd->bhd/dot_general | solution.py:94
  67.6 7.5 %all-gather.2 = f32[128,2,64]{2,1,0:T(2,128)S(1)} all-gather(f32[32,2,64]{2,1,0:T(2,128)S(1)} %bitcast.49), channel_id=4, replica_groups=mesh['kv'=4,'tp'=8] {'kv'}, dimensions={0}, use_global_device_ids=true | all-gather | bytes 81920 | tf_op jit(solution)/shard_map/all_gather | solution.py:13
  75.0 0.0 copy-start.3
  75.0 0.6 copy-done.3
  75.7 0.1 copy.34
  75.8 8.1 %all-gather.4 = f32[4,32,2]{1,2,0:T(2,128)S(1)} all-gather(f32[1,32,2]{1,2,0:T(2,128)S(1)} %bitcast.51), channel_id=3, replica_groups=mesh['kv'=4,'tp'=8] {'kv'}, dimensions={0}, use_global_device_ids=true | all-gather | bytes 1280 | tf_op jit(solution)/shard_map/all_gather | solution.py:13
  83.8 7.1 %all-gather.3 = f32[4,32,2]{1,2,0:T(2,128)S(1)} all-gather(f32[1,32,2]{1,2,0:T(2,128)S(1)} %bitcast.50), channel_id=2, replica_groups=mesh['kv'=4,'tp'=8] {'kv'}, dimensions={0}, use_global_device_ids=true | all-gather | bytes 1280 | tf_op jit(solution)/shard_map/all_gather | solution.py:13
  90.9 3.6 %while.19 = (s32[]{:T(128)}, f32[32,2]{0,1:T(2,128)S(1)}, f32[32,2]{0,1:T(2,128)S(1)}, f32[32,2,64]{2,1,0:T(2,128)S(1)}, f32[4,32,2]{1,2,0:T(2,128)S(1)}, /*inde...) while((s32[]{:T(128)}, f32[32,2]{0,1:T(2,128)S(1)}, ...), condition=%wide.region_4.5_spmd, body=%wide.region_3.4_spmd.sunk | while | flops 12677 | bytes 52887 | solution.py:18
  90.9 0.1 copy.49
  91.0 0.1 copy.50
  91.1 1.0 fusion.57
  92.2 0.1 copy.49
  92.2 0.1 copy.50
  92.3 1.0 fusion.57
  93.4 0.1 copy.49
  93.5 0.1 copy.50
  93.5 1.0 fusion.57
  94.5 0.0 copy-done.1
  94.5 0.0 copy-done.4
  94.6 0.3 fusion.4
  94.9 0.1 reshape.33
  95.0 0.1 multiply_reduce_fusion
  95.1 0.1 copy.35
  95.2 0.1 copy.36
  95.3 0.1 copy.37
  95.4 0.1 copy.38
  95.5 0.0 copy-done.2
  95.5 0.3 fusion.3
  95.8 0.1 reshape.34
  95.9 0.2 fusion.22
  96.1 0.1 reshape.32
  96.2 1.8 fusion.42
  97.9 0.0 all-reduce.3.cloned.1.call-update
  98.0 0.0 all-reduce.5.cloned.1.call-start
  98.0 0.7 dynamic_slice.59
  98.7 51.7 %all-reduce.3.cloned.1.call-done = f32[32,1024]{1,0:T(8,128)} async-done(((f32[32,1024]{1,0:T(8,128)}), f32[32,1024]{1,0:T(8,128)}) %all-reduce.3.cloned.1.call-update) | async-done | bytes 131088 | tf_op jit(solution)/shard_map/psum | solution.py:110
  150.4 1.0 fusion.13
  151.4 9.8 %psum.22 = f32[32]{0:T(128)S(1)} all-reduce(f32[32]{0:T(128)S(1)} %get-tuple-element.204), channel_id=1, replica_groups=mesh['kv'=4,'tp'=8] {'kv'}, use_global_device_ids=true, to_apply=%region_8.9 | all-reduce | flops 32 | bytes 256 | tf_op jit(solution)/shard_map/psum | solution.py:115
  161.3 3.8 %fusion.18 = f32[32,2048]{1,0:T(8,128)} fusion(bf16[1024,2048]{1,0:T(8,128)(2,1)} %param.28, bf16[32,1024]{1,0:T(8,128)(2,1)S(1)} %get-tuple-element.205, f32[1024]{0:T(1024)S(1)} %dynamic_slice.59, f32[32]{0:T(128)S(1)} %add_rsqrt_fusion), kind=kOutput, calls=%fused_computation.37 | convolution fusion | flops 134348800 | bytes 4526208 | tf_op jit(solution)/shard_map/dot_general | solution.py:126
  165.0 0.0 all-reduce.5.cloned.1.call-update
  165.1 0.0 reduce-scatter.2.cloned.1.call-start
  165.1 40.4 %all-reduce.5.cloned.1.call-done = f32[32,2048]{1,0:T(8,128)} async-done(((f32[32,2048]{1,0:T(8,128)}), f32[32,2048]{1,0:T(8,128)}) %all-reduce.5.cloned.1.call-update) | async-done | bytes 262160 | tf_op jit(solution)/shard_map/psum | solution.py:127
  205.5 3.8 %fusion.16 = f32[32,1024]{1,0:T(8,128)} fusion(bf16[2048,1024]{1,0:T(8,128)(2,1)} %param.29, f32[32,2048]{1,0:T(8,128)} %all-reduce.5.cloned.1.call-done), kind=kOutput, calls=%fused_computation.34 | convolution fusion | flops 134414336 | bytes 4587520 | tf_op jit(solution)/shard_map/dot_general | solution.py:128
  209.3 0.0 reduce-scatter.2.cloned.1.call-update
  209.3 30.7 %reduce-scatter.2.cloned.1.call-done = f32[32,128]{1,0:T(8,128)} async-done(((f32[32,1024]{1,0:T(8,128)}), f32[32,128]{1,0:T(8,128)}) %reduce-scatter.2.cloned.1.call-update) | async-done | bytes 16400 | tf_op jit(solution)/shard_map/reduce_scatter | solution.py:129
  240.0 1.3 add_convert_fusion.1
  (10 shorter events, 0.1 us)
Async XLA Ops:
  6.5 44.8 %copy-start = (bf16[4096,128]{1,0:T(8,128)(2,1)S(1)}, bf16[4096,128]{1,0:T(8,128)(2,1)}, u32[]{:S(2)}) copy-start(bf16[4096,128]{1,0:T(8,128)(2,1)} %param.18) | copy-start | bytes 3145732
  6.5 143.8 %all-reduce.3.cloned.1.call-start = ((), (), s32[]{:S(2)}) async-start(), calls=%async_computation.1 | async-start | bytes 262144 | tf_op jit(solution)/shard_map/psum | solution.py:110
  58.4 36.1 %copy-start.1 = (bf16[4096,128]{1,0:T(8,128)(2,1)S(1)}, bf16[4096,128]{1,0:T(8,128)(2,1)}, u32[]{:S(2)}) copy-start(bf16[4096,128]{1,0:T(8,128)(2,1)} %param.19) | copy-start | bytes 3145732
  58.4 36.1 %copy-start.4 = (f32[4096]{0:T(1024)S(1)}, f32[4096]{0:T(1024)}, u32[]{:S(2)}) copy-start(f32[4096]{0:T(1024)} %param.17) | copy-start | bytes 49156
  58.5 37.0 %copy-start.2 = (bf16[4096,128]{1,0:T(8,128)(2,1)S(1)}, bf16[4096,128]{1,0:T(8,128)(2,1)}, u32[]{:S(2)}) copy-start(bf16[4096,128]{1,0:T(8,128)(2,1)} %param.20) | copy-start | bytes 3145732
  75.0 0.6 copy-start.3
  98.0 107.5 %all-reduce.5.cloned.1.call-start = ((), (), s32[]{:S(2)}) async-start(), calls=%async_computation.2 | async-start | bytes 524288 | tf_op jit(solution)/shard_map/psum | solution.py:127
  165.1 75.0 %reduce-scatter.2.cloned.1.call-start = ((), (), s32[]{:S(2)}) async-start(), calls=%async_computation.3 | async-start | bytes 147456 | tf_op jit(solution)/shard_map/reduce_scatter | solution.py:129
Sparse Core Ops, SparseCore 0:
  98.1 52.2 all-reduce.2
  165.2 40.2 all-reduce.4
  209.4 30.5 reduce-scatter.1
where the time goes:
time: 249 us; the launch traced here: 248 us
  waiting for transfers between devices  123 us (49%)
  blocking collectives  77.1 us (31%)
  matrix products  22.4 us (9%)
  between operations  13.2 us (5%)
  other arithmetic  9.28 us (4%)
  local copies, waits for them, and re-layouts  2.9 us (1%)
    psum x1, waiting for transfers between devices, shards(): block_sum = lax.psum(partial_value, 'tp')  51.7 us
    all_gather x1, blocking collectives, shards(): gathered = lax.all_gather(stream, ('kv', 'tp'), axis=1, tiled=True)  44.6 us
    psum x1, waiting for transfers between devices, shards(): hidden = squared_relu(lax.psum(up_partial, 'kv'))  40.4 us
    reduce_scatter x1, waiting for transfers between devices, shards(): lax.psum_scatter(down_partial, 'tp', scatter_dimension=1, tiled=True)  30.7 us
    all_gather x3, blocking collectives, combined_all(): gathered = jax.tree.map(lambda a: lax.all_gather(a, axis), part)  22.6 us
    psum x1, blocking collectives, shards(): squares = lax.psum(row_squares(middle_block), 'kv')  9.84 us
    dot_general x1, matrix products, shards(): jnp.einsum('bhp,bhpd->bhd', weights, value_cache, preferred_element_type=...  5.65 us
  transfers between devices with their start and end apart: 3, of which 3 were waited for; matrix products, arithmetic and copies ran while one was open for 0% of the time, Pallas kernels for 0%

commit v1 on v0

--- a/solution.py
+++ b/solution.py
@@ -1,6 +1,10 @@
+import functools
+
 import jax
 import jax.numpy as jnp
 from jax import lax
+from jax.experimental import pallas as pl
+from jax.experimental.pallas import tpu as pltpu
 from jax.sharding import PartitionSpec as P
 
 D = 4096
@@ -130,26 +134,459 @@
     return (middle_piece.astype(jnp.float32) + reduced).astype(jnp.bfloat16)
 
 
+MESH = pl.DeviceIdType.MESH
+F32 = jnp.float32
+BF16 = jnp.bfloat16
+NT = (((1,), (1,)), ((), ()))
+
+
+def layer_kernel(
+    sizes,
+    stream_hbm,
+    mixer_gain,
+    query_hbm,
+    key_hbm,
+    value_hbm,
+    forget_weight,
+    forget_bias,
+    keys_hbm,
+    values_hbm,
+    decay_hbm,
+    out_hbm,
+    channel_gain,
+    up_hbm,
+    down_hbm,
+    result,
+    pieces,
+    qkv_v,
+    keys_v,
+    values_v,
+    decay_v,
+    out_v,
+    up_v,
+    down_v,
+    normed,
+    query_s,
+    forget_s,
+    parts,
+    out_parts,
+    out_got,
+    middles,
+    mixed,
+    squares,
+    up_parts,
+    up_got,
+    hidden,
+    down_sum,
+    down_parts,
+    down_got,
+    local_sem,
+    keys_sem,
+    values_sem,
+    tp_send,
+    tp_recv,
+    kv_send,
+    kv_recv,
+):
+    n_kv, n_tp, rows, width, chunk, heads, head = sizes
+    me_kv, me_tp = lax.axis_index("kv"), lax.axis_index("tp")
+    groups = rows // 8
+    group_depth = 8 * width
+    full = n_kv * n_tp * width
+    scale = float(head) ** (-0.5)
+
+    def tp_peer(step):
+        return lax.rem(me_tp + step, n_tp)
+
+    def kv_peer(step):
+        return lax.rem(me_kv + step, n_kv)
+
+    local = []
+
+    def load(source, target):
+        copy = pltpu.make_async_copy(source, target, local_sem.at[len(local)])
+        copy.start()
+        local.append(copy)
+        return copy
+
+    own_in = load(stream_hbm, pieces.at[me_kv, me_tp])
+    for step in range(1, n_tp):
+        pl.semaphore_signal(
+            pltpu.get_barrier_semaphore(), inc=1, device_id={"tp": tp_peer(step)}, device_id_type=MESH
+        )
+    for step in range(1, n_kv):
+        pl.semaphore_signal(
+            pltpu.get_barrier_semaphore(), inc=1, device_id={"kv": kv_peer(step)}, device_id_type=MESH
+        )
+    qkv_in = [
+        load(source, qkv_v.at[:, pl.ds(at * width, width)])
+        for at, source in enumerate((query_hbm, key_hbm, value_hbm))
+    ]
+    decay_in = load(decay_hbm, decay_v)
+
+    def keys_copy(group):
+        span = pl.ds(pl.multiple_of(group * group_depth, group_depth), group_depth)
+        return pltpu.make_async_copy(keys_hbm.at[span], keys_v.at[span], keys_sem.at[group])
+
+    def values_copy(group):
+        span = pl.ds(pl.multiple_of(group * group_depth, group_depth), group_depth)
+        return pltpu.make_async_copy(values_hbm.at[span], values_v.at[span], values_sem.at[group])
+
+    for group in range(groups):
+        keys_copy(group).start()
+        values_copy(group).start()
+    out_in = load(out_hbm, out_v)
+    up_in = load(up_hbm, up_v)
+    down_in = load(down_hbm, down_v)
+
+    sent = []
+
+    def send_tp(phase, step, source, target):
+        copy = pltpu.make_async_remote_copy(
+            src_ref=source,
+            dst_ref=target,
+            send_sem=tp_send.at[phase, step - 1],
+            recv_sem=tp_recv.at[phase, step - 1],
+            device_id={"tp": tp_peer(step)},
+            device_id_type=MESH,
+        )
+        copy.start()
+        sent.append(copy)
+        return copy
+
+    def send_kv(phase, step, source, target):
+        copy = pltpu.make_async_remote_copy(
+            src_ref=source,
+            dst_ref=target,
+            send_sem=kv_send.at[phase, step - 1],
+            recv_sem=kv_recv.at[phase, step - 1],
+            device_id={"kv": kv_peer(step)},
+            device_id_type=MESH,
+        )
+        copy.start()
+        sent.append(copy)
+        return copy
+
+    def arrive(copies):
+        for copy in copies:
+            copy.wait_recv()
+
+    tp_order = sorted(range(1, n_tp), key=lambda step: -min(step, n_tp - step))
+    kv_order = sorted(range(1, n_kv), key=lambda step: -step)
+
+    own_in.wait()
+    pl.semaphore_wait(pltpu.get_barrier_semaphore(), n_tp - 1 + n_kv - 1)
+
+    mine = pieces.at[me_kv, me_tp]
+    arrive([send_tp(0, step, mine, mine) for step in tp_order])
+    arrive([send_kv(0, step, pieces.at[me_kv], pieces.at[me_kv]) for step in kv_order])
+
+    total = jnp.zeros((rows, width), F32)
+    for block in range(n_kv):
+        for piece in range(n_tp):
+            wide = pieces[block, piece].astype(F32)
+            total += wide * wide
+    inverse = lax.rsqrt(jnp.sum(total, axis=1, keepdims=True) / full + EPS)
+    for block in range(n_kv):
+        for piece in range(n_tp):
+            at = block * n_tp + piece
+            wide = pieces[block, piece].astype(F32)
+            normed[:, at * width : (at + 1) * width] = (
+                wide * inverse * mixer_gain[at : at + 1, :]
+            ).astype(BF16)
+
+    logits = (
+        lax.dot_general(normed[...], forget_weight[...], NT, preferred_element_type=F32)
+        + forget_bias[...]
+    )
+    forget_all = jnp.minimum(logits, 0.0) - jnp.log1p(jnp.exp(-jnp.abs(logits)))
+    column = lax.broadcasted_iota(jnp.int32, forget_all.shape, 1)
+    for index in range(heads):
+        one = jnp.sum(
+            jnp.where(column == me_tp * heads + index, forget_all, 0.0), axis=1, keepdims=True
+        )
+        forget_s[index] = jnp.broadcast_to(one, (rows, width))
+    for copy in qkv_in:
+        copy.wait()
+    projected = jnp.dot(normed[...], qkv_v[...], preferred_element_type=F32).astype(BF16).astype(F32)
+    query = projected[:, :width]
+    key_new = projected[:, width : 2 * width]
+    value_new = projected[:, 2 * width :]
+    query_s[...] = query
+    decay_in.wait()
+
+    row16 = lax.broadcasted_iota(jnp.int32, (16, width), 0)
+    lane16 = lax.broadcasted_iota(jnp.int32, (16, width), 1)
+    head_mask = (lane16 < head) == (row16 < 8)
+    row_in_group = lax.rem(row16, 8)
+    lane8 = lax.broadcasted_iota(jnp.int32, (8, width), 1)
+
+    @pl.loop(0, groups)
+    def attend(group):
+        eight = pl.ds(pl.multiple_of(group * 8, 8), 8)
+        span = pl.ds(pl.multiple_of(group * group_depth, group_depth), group_depth)
+        some = query_s[eight, :]
+        both = jnp.where(head_mask, jnp.concatenate([some, some], axis=0), 0.0)
+        spread = jnp.concatenate(
+            [jnp.where(row_in_group == at, both, 0.0) for at in range(8)], axis=1
+        ).astype(BF16)
+        keys_copy(group).wait()
+        scores = jnp.dot(spread, keys_v[span, :], preferred_element_type=F32) * scale
+        extra = jnp.concatenate(
+            [forget_s[0, eight, :][:, :1], forget_s[1, eight, :][:, :1]], axis=0
+        )
+        decay = jnp.concatenate([decay_v[eight, 0, :], decay_v[eight, 1, :]], axis=0)
+        scores = scores + extra + decay
+        top = jnp.max(scores, axis=1, keepdims=True)
+        weight = jnp.exp(scores - top).astype(BF16)
+        count = jnp.sum(weight.astype(F32), axis=1, keepdims=True)
+        values_copy(group).wait()
+        wide = lax.dot_general(weight, values_v[span, :], NT, preferred_element_type=F32)
+        kept = jnp.zeros((16, width), F32)
+        for at in range(8):
+            kept = jnp.where(row_in_group == at, wide[:, at * width : (at + 1) * width], kept)
+        low = lane8 < head
+        parts[me_kv, 0, eight, :] = jnp.where(low, kept[:8], kept[8:])
+        tops = jnp.where(low, top[:8], top[8:])
+        counts = jnp.where(low, count[:8], count[8:])
+        parts[me_kv, 1, eight, :] = jnp.where(lax.rem(lane8, head) < head // 2, tops, counts)
+
+    copies = [send_kv(1, step, parts.at[me_kv], parts.at[me_kv]) for step in kv_order]
+    lane = lax.broadcasted_iota(jnp.int32, (rows, width), 1)
+    first = lane < head
+
+    def per_head(low_column, high_column):
+        return jnp.where(first, low_column, high_column)
+
+    product = query * key_new
+    own = (
+        per_head(
+            jnp.sum(jnp.where(first, product, 0.0), axis=1, keepdims=True),
+            jnp.sum(jnp.where(first, 0.0, product), axis=1, keepdims=True),
+        )
+        * scale
+    )
+    arrive(copies)
+    half = head // 2
+    tops, counts, sums = [], [], []
+    for block in range(n_kv):
+        stat = parts[block, 1]
+        sums.append(parts[block, 0])
+        tops.append(per_head(stat[:, :1], stat[:, head : head + 1]))
+        counts.append(per_head(stat[:, half : half + 1], stat[:, head + half : head + half + 1]))
+    peak = functools.reduce(jnp.maximum, tops, own)
+    factor = jnp.exp(own - peak)
+    numer, denom = value_new * factor, factor
+    for block in range(n_kv):
+        factor = jnp.exp(tops[block] - peak)
+        numer += sums[block] * factor
+        denom += counts[block] * factor
+    attention = (numer / denom).astype(BF16)
+
+    out_in.wait()
+    partial = jnp.dot(attention, out_v[...], preferred_element_type=F32)
+    for piece in range(n_tp):
+        out_parts[piece] = partial[:, piece * width : (piece + 1) * width]
+    copies = [
+        send_tp(1, step, out_parts.at[tp_peer(step)], out_got.at[me_tp]) for step in tp_order
+    ]
+    out_got[me_tp] = out_parts[me_tp]
+    arrive(copies)
+    total = out_got[0]
+    for piece in range(1, n_tp):
+        total += out_got[piece]
+    middle = (pieces[me_kv, me_tp].astype(F32) + total).astype(BF16)
+    middles[me_tp] = middle
+    arrive([send_tp(2, step, middles.at[me_tp], middles.at[me_tp]) for step in tp_order])
+
+    gains = channel_gain[pl.ds(pl.multiple_of(me_kv * n_tp, n_tp), n_tp), :]
+    total = jnp.zeros((rows, width), F32)
+    for piece in range(n_tp):
+        wide = middles[piece].astype(F32)
+        total += wide * wide
+        mixed[:, piece * width : (piece + 1) * width] = (
+            wide * gains[piece : piece + 1, :]
+        ).astype(BF16)
+    squares[me_kv] = jnp.broadcast_to(jnp.sum(total, axis=1, keepdims=True), (rows, width))
+    copies = [send_kv(2, step, squares.at[me_kv], squares.at[me_kv]) for step in kv_order]
+    up_in.wait()
+    for step in kv_order + [0]:
+        columns = pl.ds(pl.multiple_of(kv_peer(step) * chunk, chunk), chunk)
+        partial = jnp.dot(mixed[...], up_v[:, columns], preferred_element_type=F32)
+        if step:
+            up_parts[step - 1] = partial
+            copies.append(send_kv(3, step, up_parts.at[step - 1], up_got.at[me_kv]))
+        else:
+            up_got[me_kv] = partial
+    arrive(copies)
+    square = squares[0][:, :1]
+    total = up_got[0]
+    for block in range(1, n_kv):
+        square += squares[block][:, :1]
+        total += up_got[block]
+    kept = jnp.maximum(total * lax.rsqrt(square / full + EPS), 0.0)
+    hidden[me_kv] = (kept * kept).astype(BF16)
+    copies = {step: send_kv(4, step, hidden.at[me_kv], hidden.at[me_kv]) for step in kv_order}
+    down_in.wait()
+    for at, step in enumerate([0] + list(range(1, n_kv))):
+        source = lax.rem(me_kv + n_kv - step, n_kv)
+        if step:
+            copies[step].wait_recv()
+        depth = pl.ds(pl.multiple_of(source * chunk, chunk), chunk)
+        partial = jnp.dot(hidden[source], down_v[depth, :], preferred_element_type=F32)
+        if at == 0:
+            down_sum[...] = partial
+        else:
+            down_sum[...] += partial
+    for piece in range(n_tp):
+        down_parts[piece] = down_sum[:, piece * width : (piece + 1) * width]
+    copies = [
+        send_tp(3, step, down_parts.at[tp_peer(step)], down_got.at[me_tp]) for step in tp_order
+    ]
+    down_got[me_tp] = down_parts[me_tp]
+    arrive(copies)
+    total = down_got[0]
+    for piece in range(1, n_tp):
+        total += down_got[piece]
+    result[...] = (middle.astype(F32) + total).astype(BF16)
+    for copy in sent:
+        copy.wait_send()
+
+
+def fused_layer(
+    stream,
+    mixer_gain,
+    query_weight,
+    key_weight,
+    value_weight,
+    forget_weight,
+    forget_bias,
+    key_cache,
+    value_cache,
+    past_decay,
+    out_weight,
+    channel_gain,
+    up_weight,
+    down_weight,
+):
+    n_kv, n_tp = lax.axis_size("kv"), lax.axis_size("tp")
+    rows, width = stream.shape
+    _, heads, positions, head = key_cache.shape
+    model, units = up_weight.shape
+    chunk = units // n_kv
+    columns = n_kv * n_tp
+    sizes = (n_kv, n_tp, rows, width, chunk, heads, head)
+    flat = rows * heads * head
+    keys = jnp.transpose(key_cache, (0, 1, 3, 2)).reshape(flat, positions)
+    values = jnp.transpose(value_cache, (0, 1, 3, 2)).reshape(flat, positions)
+    in_vmem = pl.BlockSpec(memory_space=pltpu.VMEM)
+    in_hbm = pl.BlockSpec(memory_space=pl.ANY)
+    vmem = pltpu.VMEM
+    dma = pltpu.SemaphoreType.DMA
+    groups = rows // 8
+    return pl.pallas_call(
+        functools.partial(layer_kernel, sizes),
+        out_shape=jax.ShapeDtypeStruct((rows, width), BF16),
+        in_specs=[
+            in_hbm, in_vmem, in_hbm, in_hbm, in_hbm, in_vmem, in_vmem,
+            in_hbm, in_hbm, in_hbm, in_hbm, in_vmem, in_hbm, in_hbm,
+        ],
+        out_specs=in_vmem,
+        scratch_shapes=[
+            vmem((n_kv, n_tp, rows, width), BF16),
+            vmem((columns * width, 3 * width), BF16),
+            vmem((flat, positions), BF16),
+            vmem((flat, positions), BF16),
+            vmem(past_decay.shape, F32),
+            vmem(out_weight.shape, BF16),
+            vmem(up_weight.shape, BF16),
+            vmem(down_weight.shape, BF16),
+            vmem((rows, columns * width), BF16),
+            vmem((rows, width), F32),
+            vmem((heads, rows, width), F32),
+            vmem((n_kv, 2, rows, width), F32),
+            vmem((n_tp, rows, width), F32),
+            vmem((n_tp, rows, width), F32),
+            vmem((n_tp, rows, width), BF16),
+            vmem((rows, model), BF16),
+            vmem((n_kv, rows, width), F32),
+            vmem((n_kv - 1, rows, chunk), F32),
+            vmem((n_kv, rows, chunk), F32),
+            vmem((n_kv, rows, chunk), BF16),
+            vmem((rows, model), F32),
+            vmem((n_tp, rows, width), F32),
+            vmem((n_tp, rows, width), F32),
+            dma((8,)),
+            dma((groups,)),
+            dma((groups,)),
+            dma((4, n_tp - 1)),
+            dma((4, n_tp - 1)),
+            dma((5, n_kv - 1)),
+            dma((5, n_kv - 1)),
+        ],
+        compiler_params=pltpu.CompilerParams(
+            collective_id=0, has_side_effects=True, vmem_limit_bytes=60 * 1024 * 1024
+        ),
+    )(
+        stream,
+        mixer_gain.reshape(columns, width),
+        query_weight,
+        key_weight,
+        value_weight,
+        forget_weight.T,
+        forget_bias.reshape(1, -1),
+        keys,
+        values,
+        past_decay,
+        out_weight,
+        channel_gain.reshape(columns, width),
+        up_weight,
+        down_weight,
+    )
+
+
+def fits_kernel(mesh, stream, key_cache, up_weight):
+    n_kv, n_tp = mesh.shape["kv"], mesh.shape["tp"]
+    batch_rows, model = stream.shape
+    heads, positions, head = key_cache.shape[1:]
+    return (
+        model // (n_kv * n_tp) == 128
+        and heads // n_tp == 2
+        and head == 64
+        and batch_rows % 16 == 0
+        and n_tp == 8
+        and (positions // n_kv) % 128 == 0
+        and (up_weight.shape[1] // (n_tp * n_kv)) % 128 == 0
+    )
+
+
 def solution(mesh):
-    return jax.shard_map(
-        shards,
-        mesh=mesh,
-        in_specs=(
-            P(None, ("kv", "tp")),
-            P(),
-            P(None, "tp"),
-            P(None, "tp"),
-            P(None, "tp"),
-            P(),
-            P(),
-            P(None, "tp", "kv", None),
-            P(None, "tp", "kv", None),
-            P(None, "tp", "kv"),
-            P("tp", "kv"),
-            P(),
-            P("kv", "tp"),
-            P("tp", "kv"),
-        ),
-        out_specs=P(None, ("kv", "tp")),
-        check_vma=False,
-    )
+    def layer(*arrays):
+        local = fused_layer if fits_kernel(mesh, arrays[0], arrays[7], arrays[12]) else shards
+        return run(local)(*arrays)
+
+    def run(local):
+        return jax.shard_map(
+            local,
+            mesh=mesh,
+            in_specs=(
+                P(None, ("kv", "tp")),
+                P(),
+                P(None, "tp"),
+                P(None, "tp"),
+                P(None, "tp"),
+                P(),
+                P(),
+                P(None, "tp", "kv", None),
+                P(None, "tp", "kv", None),
+                P(None, "tp", "kv"),
+                P("tp", "kv"),
+                P(),
+                P("kv", "tp"),
+                P("tp", "kv"),
+            ),
+            out_specs=P(None, ("kv", "tp")),
+            check_vma=False,
+        )
+
+    return layer

time: 249 us -> 51.2 us (0.21)
  waiting for transfers between devices: 123 us -> 0 us
  blocking collectives: 77.1 us -> 0 us
  Pallas kernels: 0 us -> 49.6 us
  matrix products: 22.4 us -> 0 us
  between operations: 13.2 us -> 0.01 us
  other arithmetic: 9.28 us -> 0 us
    psum x2 -> x0, waiting for transfers between devices: 92.1 us -> none  [the longest x1 51.7 us: shards(): block_sum = lax.psum(partial_value, 'tp')]
    all_gather x4 -> x0, blocking collectives: 67.2 us -> none  [the longest x1 44.6 us: shards(): gathered = lax.all_gather(stream, ('kv', 'tp'), axis=1, tiled=True)]
    pallas_call x0 -> x1, Pallas kernels: none -> 49.6 us  [fused_layer(): pl.pallas_call(functools.partial(layer_kernel, sizes), out_shape=jax.Shap...]
    reduce_scatter x1 -> x0, waiting for transfers between devices: 30.7 us -> none  [shards(): lax.psum_scatter(down_partial, 'tp', scatter_dimension=1, tiled=True)]
    dot_general x9 -> x0, matrix products: 22.4 us -> none  [the longest x1 5.65 us: shards(): jnp.einsum('bhp,bhpd->bhd', weights, value_cache, preferred_element_type=...]
    psum x1 -> x0, blocking collectives: 9.84 us -> none  [shards(): squares = lax.psum(row_squares(middle_block), 'kv')]
    add x7 -> x0, other arithmetic: 3.05 us -> none  [the longest x3 2.97 us: merge_parts(): sums_one * factor_one[..., None] + sums_two * factor_two[..., None]]
    convert_element_type x3 -> x0, other arithmetic: 2.8 us -> none  [the longest x1 1.32 us: shards(): return (middle_piece.astype(jnp.float32) + reduced).astype(jnp.bfloat16)]
  transfers between devices with their start and end apart: 3 -> 0, of which waited for: 3 -> 0; matrix products, arithmetic and copies ran while one was open for 0% -> 0% of each run, Pallas kernels for 0% -> 0%
where the time goes in v1:
time: 51.2 us; the launch traced here: 50.9 us
  Pallas kernels  49.6 us (97%)
  local copies, waits for them, and re-layouts  1.3 us (3%)
    pallas_call x1, Pallas kernels, fused_layer(): pl.pallas_call(functools.partial(layer_kernel, sizes), out_shape=jax.Shap...  49.6 us
    unnamed x1, local copies, waits for them, and re-layouts  1.3 us

profile of v1, /device:TPU:0, one launch (start us, length us, event | category | flops | bytes accessed | tf_op | source)
XLA Modules:
  0.0 50.9 jit_solution(4959901257488657999)
XLA Ops:
  0.0 49.6 %shard_map.136 = bf16[32,128]{1,0:T(8,128)(2,1)} custom-call(bf16[32,128]{1,0:T(8,128)(2,1)} %stream_hbm.1, f32[32,128]{1,0:T(8,128)} %bitcast.13, bf16[4096,128]{1,0:T(8,128)(2,1)} %query_hbm.1, bf16[4096,128]{1,0:T(8,128)(2,1)} %key_hbm.1, bf16[4096,128]{1,0:T(8,128)(2,1)} %value_hbm.1, bf16[16,4096]{1,0:T(8,128)(2,1)} %bitcast.12, f32[1,16]{1,0:T(1,128)} %bitcast.15, ...), custom_call_target="tpu_custom_call" | custom-call | tf_op jit(solution)/shard_map/pallas_call | solution.py:487
  49.6 1.3 %copy.16 = bf16[32,128]{1,0:T(8,128)(2,1)} copy(bf16[32,128]{1,0:T(8,128)(2,1)} %shard_map.136) | data formatting | bytes 16384
